TPU v7x, 32 devices: a whole 2x2x4 slice. The times are simulated.
32 devices in a mesh: ep: 8 (over z, y), tp: 4 (over x, core).
Axes of the slice: x: 2, y: 2, z: 4, core: 2. Of those that a mesh axis runs over, the one named last changes fastest.
Arguments:
- tokens: bfloat16 [64, 1024], P('ep'), may hold values from -6 to 6
- mix_gain: float32 [1024], replicated, may hold values from 0.1 to 1.9
- w_query: bfloat16 [1024, 512], P(None, 'tp'), may hold values from -0.1875 to 0.1875
- w_key: bfloat16 [1024, 512], P(None, 'tp'), may hold values from -0.1875 to 0.1875
- w_value: bfloat16 [1024, 1024], P(None, 'tp'), may hold values from -0.1875 to 0.1875
- w_ogate: bfloat16 [1024, 1024], P(None, 'tp'), may hold values from -0.1875 to 0.1875
- w_igate: bfloat16 [1024, 4], replicated, may hold values from -0.1875 to 0.1875
- w_fgate: bfloat16 [1024, 4], replicated, may hold values from -0.1875 to 0.1875
- forget_bias: float32 [4], replicated, may hold values from -1 to 3
- head_gain: float32 [1024], P('tp'), may hold values from 0.1 to 1.9
- w_out: bfloat16 [1024, 1024], P('tp'), may hold values from -0.1875 to 0.1875
- memory: float32 [64, 4, 128, 256], P('ep', 'tp'), may hold values from -0.4 to 0.4
- normalizer: float32 [64, 4, 128], P('ep', 'tp'), may hold values from -0.4 to 0.4
- running_max: float32 [64, 4], P('ep', 'tp'), may hold values from -4 to 4
- ffn_gain: float32 [1024], replicated, may hold values from 0.1 to 1.9
- route: int32 [64, 2], replicated, may hold values from 0 to 7, all different within a row; in each aligned block of 64 rows (0 to 63, 64 to 127, ...) at most 32 rows name the same one
- route_weight: float32 [64, 2], replicated, may hold values from 0.05 to 1
- w_gate: bfloat16 [8, 1024, 512], P('ep', None, 'tp'), may hold values from -0.1875 to 0.1875
- w_up: bfloat16 [8, 1024, 512], P('ep', None, 'tp'), may hold values from -0.1875 to 0.1875
- w_down: bfloat16 [8, 512, 1024], P('ep', 'tp'), may hold values from -0.25 to 0.25
Outputs:
- mixed: bfloat16 [64, 1024], P(None, 'ep')
- new_memory: float32 [64, 4, 128, 256], P('ep', 'tp')
- new_normalizer: float32 [64, 4, 128], P('ep', 'tp')
- new_max: float32 [64, 4], P('ep', 'tp')
Inputs may be any that keep to these rules, and one draw needn't show every extreme that they name: `route`: each expert is named by at most 32 routes in all, a bound that some block reaches; the two choices of a token differ.
All inputs are finite; a program needn't handle non-finite values.
Results may differ from a plain program's by a relative error of at most 0.014.
Values may be sent and summed in bfloat16 or wider, within the bound.
No kernel may reach another device: no remote copies, remote signals or barrier semaphores. Data moves between devices by JAX's collectives and lax.ppermute only.
A program may use at most 64 MiB of HBM per device.

v0:
```python
import jax
import jax.numpy as jnp
from jax import lax
from jax.sharding import PartitionSpec as P

EXPERT_CAPACITY = 32
EPS = 1e-06


def round_trip(values):
    rounded = lax.optimization_barrier(values.astype(jnp.bfloat16))
    return rounded.astype(jnp.float32)


def norm_rows(values, gain):
    floats = values.astype(jnp.float32)
    scale = lax.rsqrt(jnp.mean(floats * floats, axis=-1, keepdims=True) + EPS)
    return (floats * scale * gain).astype(jnp.bfloat16)


def slot_targets(route, expert_count, capacity):
    flat = route.reshape(-1)
    onehot = (flat[:, None] == jnp.arange(expert_count, dtype=jnp.int32)[None, :]).astype(jnp.int32)
    before = jnp.cumsum(onehot, axis=0) - onehot
    slot = jnp.sum(before * onehot, axis=1)
    return flat * capacity + slot


def shards(
    tokens,
    mix_gain,
    w_query,
    w_key,
    w_value,
    w_ogate,
    w_igate,
    w_fgate,
    forget_bias,
    head_gain,
    w_out,
    memory,
    normalizer,
    running_max,
    ffn_gain,
    route,
    route_weight,
    w_gate,
    w_up,
    w_down,
):
    width = tokens.shape[1]
    col_count = width // lax.axis_size("ep")
    qk_dim = w_query.shape[1]
    normed = norm_rows(tokens, mix_gain)
    query = round_trip(jnp.dot(normed, w_query, preferred_element_type=jnp.float32))
    scaled_key = round_trip(
        jnp.dot(normed, w_key, preferred_element_type=jnp.float32)
    ) * qk_dim ** (-0.5)
    value = round_trip(jnp.dot(normed, w_value, preferred_element_type=jnp.float32))
    ogate = round_trip(jnp.dot(normed, w_ogate, preferred_element_type=jnp.float32))
    head_pick = (jnp.arange(w_igate.shape[1], dtype=jnp.int32) == lax.axis_index("tp")).astype(
        jnp.float32
    )
    log_in = jnp.sum(
        jnp.dot(normed, w_igate, preferred_element_type=jnp.float32) * head_pick, axis=1
    )
    forget_pre = jnp.sum(
        jnp.dot(normed, w_fgate, preferred_element_type=jnp.float32) * head_pick, axis=1
    )
    log_forget = jax.nn.log_sigmoid(forget_pre + jnp.sum(forget_bias * head_pick))
    old_max = running_max[:, 0]
    new_max = jnp.maximum(log_forget + old_max, log_in)
    keep = jnp.exp(log_forget + old_max - new_max)
    admit = jnp.exp(log_in - new_max)
    state = (
        keep[:, None, None] * memory[:, 0]
        + admit[:, None, None] * scaled_key[:, :, None] * value[:, None, :]
    )
    norm_state = keep[:, None] * normalizer[:, 0] + admit[:, None] * scaled_key
    numer = jnp.einsum("tk,tkv->tv", query, state, precision=lax.Precision.HIGHEST)
    denom = jnp.sum(query * norm_state, axis=1)
    read = numer / jnp.maximum(jnp.abs(denom), jnp.exp(-new_max))[:, None]
    scale = lax.rsqrt(jnp.mean(read * read, axis=-1, keepdims=True) + EPS)
    gated = (jax.nn.sigmoid(ogate) * read * scale * head_gain).astype(jnp.bfloat16)
    local_output = lax.psum(
        jnp.dot(gated, w_out, preferred_element_type=jnp.float32).astype(jnp.bfloat16), "tp"
    ).astype(jnp.float32)
    middle_rows = (tokens.astype(jnp.float32) + local_output).astype(jnp.bfloat16)
    middle = lax.all_to_all(middle_rows, "ep", split_axis=1, concat_axis=0, tiled=True)
    expert_count = w_gate.shape[0] * lax.axis_size("ep")
    topk_count = route.shape[1]
    targets = slot_targets(route, expert_count, EXPERT_CAPACITY)
    buffer = (
        jnp.zeros((expert_count * EXPERT_CAPACITY, col_count), jnp.bfloat16)
        .at[targets]
        .set(jnp.repeat(middle, topk_count, axis=0))
    )
    buffer = buffer.reshape(expert_count, EXPERT_CAPACITY, col_count)
    rows = lax.all_to_all(buffer, "ep", split_axis=0, concat_axis=2, tiled=True)
    rows = norm_rows(rows, ffn_gain)
    gate_v = jnp.einsum("ecd,edf->ecf", rows, w_gate, preferred_element_type=jnp.float32)
    up_v = jnp.einsum("ecd,edf->ecf", rows, w_up, preferred_element_type=jnp.float32)
    activation = (jax.nn.silu(gate_v) * up_v).astype(jnp.bfloat16)
    partial_value = jnp.einsum(
        "ecf,efd->ecd", activation, w_down, preferred_element_type=jnp.float32
    )
    results = lax.psum(partial_value.astype(jnp.bfloat16), "tp")
    returned = lax.all_to_all(results, "ep", split_axis=2, concat_axis=0, tiled=True)
    picked = returned.reshape(expert_count * EXPERT_CAPACITY, col_count)[targets]
    picked = picked.reshape(route.shape[0], topk_count, col_count).astype(jnp.float32)
    weights = route_weight / jnp.sum(route_weight, axis=1, keepdims=True)
    mixed = (middle.astype(jnp.float32) + jnp.sum(picked * weights[:, :, None], axis=1)).astype(
        jnp.bfloat16
    )
    return (mixed, state[:, None], norm_state[:, None], new_max[:, None])


def solution(mesh):
    return jax.shard_map(
        shards,
        mesh=mesh,
        in_specs=(
            P("ep", None),
            P(),
            P(None, "tp"),
            P(None, "tp"),
            P(None, "tp"),
            P(None, "tp"),
            P(),
            P(),
            P(),
            P("tp"),
            P("tp", None),
            P("ep", "tp", None, None),
            P("ep", "tp", None),
            P("ep", "tp"),
            P(),
            P(),
            P(),
            P("ep", None, "tp"),
            P("ep", None, "tp"),
            P("ep", "tp", None),
        ),
        out_specs=(P(None, "ep"), P("ep", "tp", None, None), P("ep", "tp", None), P("ep", "tp")),
        check_vma=False,
    )
```

profile of v0, /device:TPU:0, one launch (start us, length us, event | category | flops | bytes accessed | tf_op | source)
XLA Modules:
  0.0 114.8 jit_solution(4171381798939121330)
XLA Ops:
  7.2 1.4 %fusion.48 = f32[]{:T(128)} fusion(f32[4]{0:T(128)} %param.28, s32[]{:T(128)S(6)} %axis_index.12), kind=kLoop, calls=%fused_computation.81 | loop fusion | flops 11 | bytes 24 | tf_op jit(solution)/shard_map/reduce_sum | solution.py:70
  8.7 0.8 fusion.28
  9.5 0.9 fusion.3
  10.4 0.9 fusion.2
  11.3 1.3 %fusion.46 = (f32[8]{0:T(128)S(1)}, f32[8]{0:T(128)S(1)}) fusion(f32[8]{0:T(128)S(1)} %fusion.3, f32[8,1]{0,1:T(1,128)} %param.33, f32[8]{0:T(128)S(1)} %fusion.2, f32[]{:T(128)} %fusion.48), kind=kLoop, calls=%fused_computation.79 | loop fusion | flops 96 | bytes 164 | tf_op jit(solution)/shard_map/exp | solution.py:73
  12.7 1.3 %exponential_bitcast_fusion = (f32[8]{0:T(128)S(1)}, f32[8,1]{0,1:T(1,128)S(1)}) fusion(f32[8]{0:T(128)S(1)} %fusion.3, f32[8,1]{0,1:T(1,128)} %param.33, f32[8]{0:T(128)S(1)} %fusion.2, f32[]{:T(128)} %fusion.48), kind=kLoop, calls=%fused_computation.104 | loop fusion | flops 96 | bytes 164 | tf_op jit(solution)/shard_map/mul | solution.py:79
  14.1 0.9 convolution_convert_fusion.5
  14.9 1.2 %convolution_convert_fusion.4 = bf16[8,128]{1,0:T(8,128)(2,1)S(1)} fusion(bf16[1024,128]{1,0:T(8,128)(2,1)} %param.23, bf16[8,1024]{1,0:T(8,128)(2,1)S(1)} %copy-done.3, f32[1024]{0:T(1024)} %param.21, f32[8]{0:T(128)S(1)} %add_rsqrt_fusion.2), kind=kOutput, calls=%fused_computation.9 | convolution fusion | flops 2130944 | bytes 284704 | tf_op jit(solution)/shard_map/dot_general | solution.py:57
  16.1 0.9 convolution_convert_fusion.2
  17.0 1.3 %convolution_convert_fusion.3 = bf16[8,256]{1,0:T(8,128)(2,1)S(1)} fusion(bf16[1024,256]{1,0:T(8,128)(2,1)} %param.25, bf16[8,1024]{1,0:T(8,128)(2,1)S(1)} %copy-done.3, f32[1024]{0:T(1024)} %param.21, f32[8]{0:T(128)S(1)} %add_rsqrt_fusion.2), kind=kOutput, calls=%fused_computation.8 | convolution fusion | flops 4229120 | bytes 548896 | tf_op jit(solution)/shard_map/dot_general | solution.py:60
  18.3 0.7 copy-done.10
  19.0 0.8 multiply_reduce_fusion.1
  19.8 0.6 fusion.5
  20.6 0.7 copy-done.13
  21.5 12.7 %psum.14 = bf16[8,1024]{1,0:T(8,128)(2,1)S(1)} all-reduce(bf16[8,1024]{1,0:T(8,128)(2,1)S(1)} %convolution_convert_fusion.1), channel_id=1, replica_groups=mesh['ep'=8,'tp'=4] {'tp'}, use_global_device_ids=true, to_apply=%region_6.7 | all-reduce | flops 8192 | bytes 32768 | tf_op jit(solution)/shard_map/psum | solution.py:85
  34.2 0.6 fusion.34
  34.8 6.0 %all-to-all-start = ((bf16[8,8,128]{2,0,1:T(8,128)(2,1)}), bf16[8,8,128]{2,0,1:T(8,128)(2,1)S(1)}, u32[]{:S(2)}, u32[]{:S(2)}) async-start(bf16[8,8,128]{2,0,1:T(8,128)(2,1)} %fusion.34), calls=%async_computation | async-start | bytes 32768 | tf_op jit(solution)/shard_map/all_to_all | solution.py:89
  41.8 5.6 %all-to-all-done = bf16[8,8,128]{2,0,1:T(8,128)(2,1)S(1)} async-done(((bf16[8,8,128]{2,0,1:T(8,128)(2,1)}), bf16[8,8,128]{2,0,1:T(8,128)(2,1)S(1)}, u32[]{:S(2)}, u32[]{:S(2)}) %all-to-all-start) | async-done | bytes 16416 | tf_op jit(solution)/shard_map/all_to_all | solution.py:89
  47.4 0.9 scatter_custom_fusion
  48.3 9.3 %all_to_all.43 = bf16[8,32,128]{2,1,0:T(8,128)(2,1)S(1)} all-to-all(bf16[8,32,128]{2,1,0:T(8,128)(2,1)S(1)} %bitcast.126), channel_id=1, replica_groups=mesh['ep'=8,'tp'=4] {'ep'}, dimensions={0} | all-to-all | bytes 131072 | tf_op jit(solution)/shard_map/all_to_all | solution.py:99
  57.7 0.6 copy-done.7
  58.6 0.6 copy-done.6
  59.3 0.9 fusion
  60.3 1.2 %multiply_add_fusion = f32[8,1,128,256]{3,2,1,0:T(8,128)} fusion(f32[8,1,128,256]{3,2,1,0:T(8,128)S(1)} %copy-done.1, f32[8,256]{1,0:T(8,128)S(1)} %convert_element_type.117, f32[8,128]{1,0:T(8,128)S(1)} %get-tuple-element.30, f32[8]{0:T(128)S(1)} %get-tuple-element.24), kind=kLoop, calls=%fused_computation.18 | loop fusion | flops 786432 | bytes 2109472 | tf_op jit(solution)/shard_map/add | solution.py:76
  61.5 27.0 %all-reduce.2.cloned.1.call-done = bf16[1,32,1024]{2,1,0:T(8,128)(2,1)} async-done(((bf16[1,32,1024]{2,1,0:T(8,128)(2,1)}), bf16[1,32,1024]{2,1,0:T(8,128)(2,1)}) %all-reduce.2.cloned.1.call-update) | async-done | bytes 65552 | tf_op jit(solution)/shard_map/psum | solution.py:107
  88.5 1.1 copy.50
  90.1 2.3 %reduce.3 = bf16[1024,32]{1,0:T(8,128)(2,1)S(1)} reduce(bf16[1024,1,32]{2,1,0:T(2,128)(2,1)S(1)} %bitcast.121, bf16[]{:T(256)} %broadcast.215), dimensions={1}, to_apply=%bitcast.105.reduce_sub_computation | reduce | bytes 131074
  92.4 0.9 reshape.303
  93.3 5.5 %all-to-all-start.2 = ((bf16[8,2,2048]{2,1,0:T(2,128)(2,1)}), bf16[8,2,2048]{2,1,0:T(2,128)(2,1)S(1)}, u32[]{:S(2)}, u32[]{:S(2)}) async-start(bf16[8,2,2048]{2,1,0:T(2,128)(2,1)} %reshape.303), calls=%async_computation.2 | async-start | bytes 131072 | tf_op jit(solution)/shard_map/all_to_all | solution.py:108
  99.0 6.8 %all-to-all-done.2 = bf16[8,2,2048]{2,1,0:T(2,128)(2,1)S(1)} async-done(((bf16[8,2,2048]{2,1,0:T(2,128)(2,1)}), bf16[8,2,2048]{2,1,0:T(2,128)(2,1)S(1)}, u32[]{:S(2)}, u32[]{:S(2)}) %all-to-all-start.2) | async-done | bytes 65568 | tf_op jit(solution)/shard_map/all_to_all | solution.py:108
  106.4 0.7 gather_fusion
  107.3 0.6 add_convert_fusion
  (61 shorter events, 3.4 us)
Async XLA Ops:
  7.2 13.5 %copy-start = (bf16[256,1024]{1,0:T(8,128)(2,1)S(1)}, bf16[256,1024]{1,0:T(8,128)(2,1)}, u32[]{:S(2)}) copy-start(bf16[256,1024]{1,0:T(8,128)(2,1)} %param.30) | copy-start | bytes 1572868
  7.2 2.3 %copy-start.3 = (bf16[8,1024]{1,0:T(8,128)(2,1)S(1)}, bf16[8,1024]{1,0:T(8,128)(2,1)}, u32[]{:S(2)}) copy-start(bf16[8,1024]{1,0:T(8,128)(2,1)} %param.20) | copy-start | bytes 49156
  7.2 6.8 %copy-start.12 = (bf16[1024,128]{1,0:T(8,128)(2,1)S(1)}, bf16[1024,128]{1,0:T(8,128)(2,1)}, u32[]{:S(2)}) copy-start(bf16[1024,128]{1,0:T(8,128)(2,1)} %param.22) | copy-start | bytes 786436
  7.2 8.9 %copy-start.2 = (bf16[1024,256]{1,0:T(8,128)(2,1)S(1)}, bf16[1024,256]{1,0:T(8,128)(2,1)}, u32[]{:S(2)}) copy-start(bf16[1024,256]{1,0:T(8,128)(2,1)} %param.24) | copy-start | bytes 1572868
  7.2 12.6 %copy-start.1 = (f32[8,1,128,256]{3,2,1,0:T(8,128)S(1)}, f32[8,1,128,256]{3,2,1,0:T(8,128)}, u32[]{:S(2)}) copy-start(f32[8,1,128,256]{3,2,1,0:T(8,128)} %param.31) | copy-start | bytes 3145732
  14.0 5.8 %copy-start.11 = (f32[8,1]{0,1:T(1,128)}, f32[8,1]{0,1:T(1,128)S(1)}, u32[]{:S(2)}) copy-start(f32[8,1]{0,1:T(1,128)S(1)} %get-tuple-element.29) | copy-start | bytes 100
  18.3 0.7 copy-start.10
  20.6 0.7 copy-start.13
  34.8 6.0 %copy-start.8 = (s32[64,2]{0,1:T(2,128)S(1)}, s32[64,2]{0,1:T(2,128)}, u32[]{:S(2)}) copy-start(s32[64,2]{0,1:T(2,128)} %param.35) | copy-start | bytes 1540
  34.8 12.5 %all-to-all-start = ((bf16[8,8,128]{2,0,1:T(8,128)(2,1)}), bf16[8,8,128]{2,0,1:T(8,128)(2,1)S(1)}, u32[]{:S(2)}, u32[]{:S(2)}) async-start(bf16[8,8,128]{2,0,1:T(8,128)(2,1)} %fusion.34), calls=%async_computation | async-start | bytes 32768 | tf_op jit(solution)/shard_map/all_to_all | solution.py:89
  40.8 47.7 %all-reduce.2.cloned.1.call-start = ((), (), s32[]{:S(2)}) async-start(), calls=%async_computation.3 | async-start | bytes 131072 | tf_op jit(solution)/shard_map/psum | solution.py:107
  47.4 11.0 %copy-start.4 = (bf16[1,1024,128]{2,1,0:T(8,128)(2,1)S(1)}, bf16[1,1024,128]{2,1,0:T(8,128)(2,1)}, u32[]{:S(2)}) copy-start(bf16[1,1024,128]{2,1,0:T(8,128)(2,1)} %param.37) | copy-start | bytes 786436
  57.6 0.7 copy-start.7
  58.3 0.9 copy-start.6
  58.4 1.0 copy-start.5
  60.3 1.2 %copy-start.9 = (f32[64,2]{0,1:T(2,128)S(1)}, f32[64,2]{0,1:T(2,128)}, u32[]{:S(2)}) copy-start(f32[64,2]{0,1:T(2,128)} %param.36) | copy-start | bytes 1540
  93.3 12.4 %all-to-all-start.2 = ((bf16[8,2,2048]{2,1,0:T(2,128)(2,1)}), bf16[8,2,2048]{2,1,0:T(2,128)(2,1)S(1)}, u32[]{:S(2)}, u32[]{:S(2)}) async-start(bf16[8,2,2048]{2,1,0:T(2,128)(2,1)} %reshape.303), calls=%async_computation.2 | async-start | bytes 131072 | tf_op jit(solution)/shard_map/all_to_all | solution.py:108
Sparse Core Ops, SparseCore 0:
  60.4 28.0 all-reduce.1
where the time goes:
time: 116 us; the launch traced here: 115 us
  waiting for transfers between devices  39.4 us (34%)
  blocking collectives  22 us (19%)
  between operations  14.3 us (12%)
  starting transfers between devices  11.5 us (10%)
  other arithmetic  11.4 us (10%)
  local copies, waits for them, and re-layouts  8.14 us (7%)
  matrix products  7.98 us (7%)
    psum x1, waiting for transfers between devices, shards(): results = lax.psum(partial_value.astype(jnp.bfloat16), 'tp')  27 us
    psum x1, blocking collectives, shards(): lax.psum(jnp.dot(gated, w_out, preferred_element_type=jnp.float32).astype...  12.7 us
    all_to_all x1, blocking collectives, shards(): rows = lax.all_to_all(buffer, 'ep', split_axis=0, concat_axis=2, tiled=True)  9.29 us
    all_to_all x1, waiting for transfers between devices, shards(): lax.all_to_all(results, 'ep', split_axis=2, concat_axis=0, tiled=True)  6.79 us
    all_to_all x1, starting transfers between devices, shards(): lax.all_to_all(middle_rows, 'ep', split_axis=1, concat_axis=0, tiled=True)  5.97 us
    all_to_all x1, waiting for transfers between devices, shards(): lax.all_to_all(middle_rows, 'ep', split_axis=1, concat_axis=0, tiled=True)  5.58 us
    all_to_all x1, starting transfers between devices, shards(): lax.all_to_all(results, 'ep', split_axis=2, concat_axis=0, tiled=True)  5.52 us
    unnamed x33, local copies, waits for them, and re-layouts  4.59 us
  transfers between devices with their start and end apart: 3, of which 3 were waited for; matrix products, arithmetic and copies ran while one was open for 2% of the time, Pallas kernels for 0%

commit v1 on v0

--- a/solution.py
+++ b/solution.py
@@ -104,7 +104,9 @@
     partial_value = jnp.einsum(
         "ecf,efd->ecd", activation, w_down, preferred_element_type=jnp.float32
     )
-    results = lax.psum(partial_value.astype(jnp.bfloat16), "tp")
+    part = partial_value.astype(jnp.bfloat16)
+    shards_2 = lax.all_gather(part, "tp", axis=0, tiled=False)
+    results = shards_2.sum(axis=0)
     returned = lax.all_to_all(results, "ep", split_axis=2, concat_axis=0, tiled=True)
     picked = returned.reshape(expert_count * EXPERT_CAPACITY, col_count)[targets]
     picked = picked.reshape(route.shape[0], topk_count, col_count).astype(jnp.float32)

time: 116 us -> 77.2 us (0.67)
  waiting for transfers between devices: 39.4 us -> 17.9 us
  between operations: 14.3 us -> 0.98 us
  blocking collectives: 22 us -> 18.5 us
  starting transfers between devices: 11.5 us -> 12.7 us
    psum x1 -> x0, waiting for transfers between devices: 27 us -> none  [shards(): results = lax.psum(partial_value.astype(jnp.bfloat16), 'tp')]
    all_to_all x1 -> x0, blocking collectives: 9.29 us -> none  [shards(): rows = lax.all_to_all(buffer, 'ep', split_axis=0, concat_axis=2, tiled=True)]
    all_gather x0 -> x1, blocking collectives: none -> 5.78 us  [shards(): shards_2 = lax.all_gather(part, 'tp', axis=0, tiled=False)]
    all_to_all x0 -> x1, waiting for transfers between devices: none -> 5.59 us  [shards(): rows = lax.all_to_all(buffer, 'ep', split_axis=0, concat_axis=2, tiled=True)]
    all_to_all x0 -> x1, starting transfers between devices: none -> 3.35 us  [shards(): rows = lax.all_to_all(buffer, 'ep', split_axis=0, concat_axis=2, tiled=True)]
    all_to_all x1, starting transfers between devices: 5.52 us -> 3.35 us  [shards(): lax.all_to_all(results, 'ep', split_axis=2, concat_axis=0, tiled=True)]
  transfers between devices with their start and end apart: 3 -> 3, of which waited for: 3 -> 3; matrix products, arithmetic and copies ran while one was open for 2% -> 3% of each run, Pallas kernels for 0% -> 0%
where the time goes in v1:
time: 77.2 us; the launch traced here: 76.3 us
  blocking collectives  18.5 us (24%)
  waiting for transfers between devices  17.9 us (23%)
  starting transfers between devices  12.7 us (16%)
  other arithmetic  11.5 us (15%)
  local copies, waits for them, and re-layouts  7.39 us (10%)
  matrix products  7.34 us (10%)
  between operations  0.98 us (1%)
    psum x1, blocking collectives, shards(): lax.psum(jnp.dot(gated, w_out, preferred_element_type=jnp.float32).astype...  12.7 us
    all_to_all x1, waiting for transfers between devices, shards(): lax.all_to_all(results, 'ep', split_axis=2, concat_axis=0, tiled=True)  6.73 us
    all_to_all x1, starting transfers between devices, shards(): lax.all_to_all(middle_rows, 'ep', split_axis=1, concat_axis=0, tiled=True)  5.97 us
    all_gather x1, blocking collectives, shards(): shards_2 = lax.all_gather(part, 'tp', axis=0, tiled=False)  5.78 us
    all_to_all x1, waiting for transfers between devices, shards(): lax.all_to_all(middle_rows, 'ep', split_axis=1, concat_axis=0, tiled=True)  5.63 us
    all_to_all x1, waiting for transfers between devices, shards(): rows = lax.all_to_all(buffer, 'ep', split_axis=0, concat_axis=2, tiled=True)  5.59 us
    unnamed x33, local copies, waits for them, and re-layouts  4.02 us
    all_to_all x1, starting transfers between devices, shards(): rows = lax.all_to_all(buffer, 'ep', split_axis=0, concat_axis=2, tiled=True)  3.35 us
  transfers between devices with their start and end apart: 3, of which 3 were waited for; matrix products, arithmetic and copies ran while one was open for 3% of the time, Pallas kernels for 0%

profile of v1, /device:TPU:0, one launch (start us, length us, event | category | flops | bytes accessed | tf_op | source)
XLA Modules:
  0.0 76.3 jit_solution(18295127185329042904)
XLA Ops:
  0.7 1.4 %fusion.47 = f32[]{:T(128)} fusion(f32[4]{0:T(128)} %param.28, s32[]{:T(128)S(6)} %axis_index.12), kind=kLoop, calls=%fused_computation.80 | loop fusion | flops 11 | bytes 24 | tf_op jit(solution)/shard_map/reduce_sum | solution.py:70
  2.1 0.8 %fusion.27 = f32[8]{0:T(128)S(1)} fusion(bf16[8,1024]{1,0:T(8,128)(2,1)} %param.20), kind=kLoop, calls=%fused_computation.45 | loop fusion | flops 24568 | bytes 16416 | tf_op jit(solution)/shard_map/reduce_sum | solution.py:17
  3.0 0.9 %fusion.2 = f32[8]{0:T(128)S(1)} fusion(bf16[1024,4]{0,1:T(4,128)(2,1)} %param.26, f32[4]{0:T(128)S(1)} %compare_convert_fusion, bf16[8,1024]{1,0:T(8,128)(2,1)S(1)} %copy-done.3, f32[1024]{0:T(1024)} %param.21, f32[8]{0:T(128)S(1)} %add_rsqrt_fusion.2), kind=kOutput, calls=%fused_computation.13 | convolution fusion | flops 98360 | bytes 28752 | tf_op jit(solution)/shard_map/dot_general | solution.py:65
  3.9 0.9 %fusion.1 = f32[8]{0:T(128)S(1)} fusion(bf16[1024,4]{0,1:T(4,128)(2,1)} %param.27, f32[4]{0:T(128)S(1)} %compare_convert_fusion, bf16[8,1024]{1,0:T(8,128)(2,1)S(1)} %copy-done.3, f32[1024]{0:T(1024)} %param.21, f32[8]{0:T(128)S(1)} %add_rsqrt_fusion.2), kind=kOutput, calls=%fused_computation.12 | convolution fusion | flops 98360 | bytes 28752 | tf_op jit(solution)/shard_map/dot_general | solution.py:68
  4.8 1.3 %fusion.45 = (f32[8]{0:T(128)S(1)}, f32[8]{0:T(128)S(1)}) fusion(f32[8]{0:T(128)S(1)} %fusion.2, f32[8,1]{0,1:T(1,128)} %param.33, f32[8]{0:T(128)S(1)} %fusion.1, f32[]{:T(128)} %fusion.47), kind=kLoop, calls=%fused_computation.78 | loop fusion | flops 96 | bytes 164 | tf_op jit(solution)/shard_map/exp | solution.py:73
  6.1 1.3 %exponential_bitcast_fusion = (f32[8]{0:T(128)S(1)}, f32[8,1]{0,1:T(1,128)S(1)}) fusion(f32[8]{0:T(128)S(1)} %fusion.2, f32[8,1]{0,1:T(1,128)} %param.33, f32[8]{0:T(128)S(1)} %fusion.1, f32[]{:T(128)} %fusion.47), kind=kLoop, calls=%fused_computation.103 | loop fusion | flops 96 | bytes 164 | tf_op jit(solution)/shard_map/mul | solution.py:79
  7.5 0.9 %convolution_convert_fusion.5 = bf16[8,128]{1,0:T(8,128)(2,1)S(1)} fusion(bf16[1024,128]{1,0:T(8,128)(2,1)S(1)} %copy-done.12, bf16[8,1024]{1,0:T(8,128)(2,1)S(1)} %copy-done.3, f32[1024]{0:T(1024)} %param.21, f32[8]{0:T(128)S(1)} %add_rsqrt_fusion.2), kind=kOutput, calls=%fused_computation.9 | convolution fusion | flops 2130944 | bytes 284704 | tf_op jit(solution)/shard_map/dot_general | solution.py:55
  8.4 1.2 %convolution_convert_fusion.4 = bf16[8,128]{1,0:T(8,128)(2,1)S(1)} fusion(bf16[1024,128]{1,0:T(8,128)(2,1)} %param.23, bf16[8,1024]{1,0:T(8,128)(2,1)S(1)} %copy-done.3, f32[1024]{0:T(1024)} %param.21, f32[8]{0:T(128)S(1)} %add_rsqrt_fusion.2), kind=kOutput, calls=%fused_computation.8 | convolution fusion | flops 2130944 | bytes 284704 | tf_op jit(solution)/shard_map/dot_general | solution.py:57
  9.6 0.9 %convolution_convert_fusion.2 = bf16[8,256]{1,0:T(8,128)(2,1)S(1)} fusion(bf16[1024,256]{1,0:T(8,128)(2,1)S(1)} %copy-done.2, bf16[8,1024]{1,0:T(8,128)(2,1)S(1)} %copy-done.3, f32[1024]{0:T(1024)} %param.21, f32[8]{0:T(128)S(1)} %add_rsqrt_fusion.2), kind=kOutput, calls=%fused_computation.6 | convolution fusion | flops 4229120 | bytes 548896 | tf_op jit(solution)/shard_map/dot_general | solution.py:59
  10.5 1.3 %convolution_convert_fusion.3 = bf16[8,256]{1,0:T(8,128)(2,1)S(1)} fusion(bf16[1024,256]{1,0:T(8,128)(2,1)} %param.25, bf16[8,1024]{1,0:T(8,128)(2,1)S(1)} %copy-done.3, f32[1024]{0:T(1024)} %param.21, f32[8]{0:T(128)S(1)} %add_rsqrt_fusion.2), kind=kOutput, calls=%fused_computation.7 | convolution fusion | flops 4229120 | bytes 548896 | tf_op jit(solution)/shard_map/dot_general | solution.py:60
  11.8 0.7 copy-done.10
  12.5 0.8 %multiply_reduce_fusion.1 = (f32[8]{0:T(128)S(1)}, f32[8,128]{1,0:T(8,128)}, f32[8,128]{1,0:T(8,128)S(1)}) fusion(bf16[8,128]{1,0:T(8,128)(2,1)S(1)} %convolution_convert_fusion.5, f32[8]{0:T(128)S(1)} %fusion.60, bf16[8,128]{1,0:T(8,128)(2,1)S(1)} %convolution_convert_fusion.4, f32[8,128]{1,0:T(8,128)S(1)} %bitcast.134, f32[8]{0:T(128)S(1)} %get-tuple-element.28, ...), kind=kLoop, calls=%fused_computation.69 | loop fusion | flops 8184 | bytes 16512 | tf_op jit(solution)/shard_map/reduce_sum | solution.py:81
  13.3 0.6 fusion.4
  14.1 0.7 copy-done.13
  15.0 12.7 %psum.7 = bf16[8,1024]{1,0:T(8,128)(2,1)S(1)} all-reduce(bf16[8,1024]{1,0:T(8,128)(2,1)S(1)} %convolution_convert_fusion.1), channel_id=1, replica_groups=mesh['ep'=8,'tp'=4] {'tp'}, use_global_device_ids=true, to_apply=%region_6.7 | all-reduce | flops 8192 | bytes 32768 | tf_op jit(solution)/shard_map/psum | solution.py:85
  27.7 0.6 fusion.33
  28.3 6.0 %all-to-all-start = ((bf16[8,8,128]{2,0,1:T(8,128)(2,1)}), bf16[8,8,128]{2,0,1:T(8,128)(2,1)S(1)}, u32[]{:S(2)}, u32[]{:S(2)}) async-start(bf16[8,8,128]{2,0,1:T(8,128)(2,1)} %fusion.33), calls=%async_computation | async-start | bytes 32768 | tf_op jit(solution)/shard_map/all_to_all | solution.py:89
  35.2 5.6 %all-to-all-done = bf16[8,8,128]{2,0,1:T(8,128)(2,1)S(1)} async-done(((bf16[8,8,128]{2,0,1:T(8,128)(2,1)}), bf16[8,8,128]{2,0,1:T(8,128)(2,1)S(1)}, u32[]{:S(2)}, u32[]{:S(2)}) %all-to-all-start) | async-done | bytes 16416 | tf_op jit(solution)/shard_map/all_to_all | solution.py:89
  40.8 1.5 %scatter_custom_fusion = bf16[256,128]{1,0:T(8,128)(2,1)} fusion(s32[128]{0:T(128)S(1)} %fusion.52, bf16[128,128]{1,0:T(8,128)(2,1)S(1)} %bitcast.131, bf16[]{:T(256)} %constant.37.clone.1), kind=kCustom, calls=%fused_computation.50 | custom fusion | bytes 65538 | tf_op jit(solution)/shard_map/scatter | solution.py:96
  42.3 3.3 %all-to-all-start.1 = ((bf16[8,32,128]{2,1,0:T(8,128)(2,1)}), bf16[8,32,128]{2,1,0:T(8,128)(2,1)S(1)}, u32[]{:S(2)}, u32[]{:S(2)}) async-start(bf16[8,32,128]{2,1,0:T(8,128)(2,1)} %bitcast.18), calls=%async_computation.1 | async-start | bytes 131072 | tf_op jit(solution)/shard_map/all_to_all | solution.py:99
  45.7 1.2 %multiply_add_fusion = f32[8,1,128,256]{3,2,1,0:T(8,128)} fusion(f32[8,1,128,256]{3,2,1,0:T(8,128)S(1)} %copy-done.1, f32[8,256]{1,0:T(8,128)S(1)} %convert_element_type.117, f32[8,128]{1,0:T(8,128)S(1)} %get-tuple-element.30, f32[8]{0:T(128)S(1)} %get-tuple-element.24), kind=kLoop, calls=%fused_computation.17 | loop fusion | flops 786432 | bytes 2109472 | tf_op jit(solution)/shard_map/add | solution.py:76
  46.9 5.6 %all-to-all-done.1 = bf16[8,32,128]{2,1,0:T(8,128)(2,1)S(1)} async-done(((bf16[8,32,128]{2,1,0:T(8,128)(2,1)}), bf16[8,32,128]{2,1,0:T(8,128)(2,1)S(1)}, u32[]{:S(2)}, u32[]{:S(2)}) %all-to-all-start.1) | async-done | bytes 65568 | tf_op jit(solution)/shard_map/all_to_all | solution.py:99
  53.0 0.7 copy-done.5
  54.0 5.8 %all-gather = bf16[128,1024]{1,0:T(8,128)(2,1)S(1)} all-gather(bf16[32,1024]{1,0:T(8,128)(2,1)S(1)} %convolution_convert_fusion), channel_id=2, replica_groups=mesh['ep'=8,'tp'=4] {'tp'}, dimensions={0}, use_global_device_ids=true | all-gather | bytes 327680 | tf_op jit(solution)/shard_map/all_gather | solution.py:108
  59.8 0.4 copy.49
  60.2 0.5 broadcast.215
  60.7 2.3 %reduce.6 = bf16[1024,32]{1,0:T(8,128)(2,1)S(1)} reduce(bf16[1024,1,32]{2,1,0:T(2,128)(2,1)S(1)} %bitcast.121, bf16[]{:T(256)} %broadcast.215), dimensions={1}, to_apply=%bitcast.105.reduce_sub_computation | reduce | bytes 131074
  63.0 0.9 %reshape.307 = bf16[8,2,2048]{2,1,0:T(2,128)(2,1)} reshape(bf16[1024,32]{1,0:T(8,128)(2,1)S(1)} %reduce.6) | data formatting | bytes 131072
  63.9 3.3 %all-to-all-start.2 = ((bf16[8,2,2048]{2,1,0:T(2,128)(2,1)}), bf16[8,2,2048]{2,1,0:T(2,128)(2,1)S(1)}, u32[]{:S(2)}, u32[]{:S(2)}) async-start(bf16[8,2,2048]{2,1,0:T(2,128)(2,1)} %reshape.307), calls=%async_computation.2 | async-start | bytes 131072 | tf_op jit(solution)/shard_map/all_to_all | solution.py:110
  67.4 6.7 %all-to-all-done.2 = bf16[8,2,2048]{2,1,0:T(2,128)(2,1)S(1)} async-done(((bf16[8,2,2048]{2,1,0:T(2,128)(2,1)}), bf16[8,2,2048]{2,1,0:T(2,128)(2,1)S(1)}, u32[]{:S(2)}, u32[]{:S(2)}) %all-to-all-start.2) | async-done | bytes 65568 | tf_op jit(solution)/shard_map/all_to_all | solution.py:110
  74.8 0.7 gather_fusion
  75.7 0.6 add_convert_fusion
  (61 shorter events, 3.1 us)
Async XLA Ops:
  0.6 13.5 %copy-start = (bf16[256,1024]{1,0:T(8,128)(2,1)S(1)}, bf16[256,1024]{1,0:T(8,128)(2,1)}, u32[]{:S(2)}) copy-start(bf16[256,1024]{1,0:T(8,128)(2,1)} %param.30) | copy-start | bytes 1572868
  0.6 2.3 %copy-start.3 = (bf16[8,1024]{1,0:T(8,128)(2,1)S(1)}, bf16[8,1024]{1,0:T(8,128)(2,1)}, u32[]{:S(2)}) copy-start(bf16[8,1024]{1,0:T(8,128)(2,1)} %param.20) | copy-start | bytes 49156
  0.7 6.8 %copy-start.12 = (bf16[1024,128]{1,0:T(8,128)(2,1)S(1)}, bf16[1024,128]{1,0:T(8,128)(2,1)}, u32[]{:S(2)}) copy-start(bf16[1024,128]{1,0:T(8,128)(2,1)} %param.22) | copy-start | bytes 786436
  0.7 8.9 %copy-start.2 = (bf16[1024,256]{1,0:T(8,128)(2,1)S(1)}, bf16[1024,256]{1,0:T(8,128)(2,1)}, u32[]{:S(2)}) copy-start(bf16[1024,256]{1,0:T(8,128)(2,1)} %param.24) | copy-start | bytes 1572868
  0.7 12.6 %copy-start.1 = (f32[8,1,128,256]{3,2,1,0:T(8,128)S(1)}, f32[8,1,128,256]{3,2,1,0:T(8,128)}, u32[]{:S(2)}) copy-start(f32[8,1,128,256]{3,2,1,0:T(8,128)} %param.31) | copy-start | bytes 3145732
  7.5 5.8 %copy-start.11 = (f32[8,1]{0,1:T(1,128)}, f32[8,1]{0,1:T(1,128)S(1)}, u32[]{:S(2)}) copy-start(f32[8,1]{0,1:T(1,128)S(1)} %get-tuple-element.29) | copy-start | bytes 100
  11.8 0.7 copy-start.10
  14.1 0.7 copy-start.13
  28.3 6.0 %copy-start.8 = (s32[64,2]{0,1:T(2,128)S(1)}, s32[64,2]{0,1:T(2,128)}, u32[]{:S(2)}) copy-start(s32[64,2]{0,1:T(2,128)} %param.35) | copy-start | bytes 1540
  28.3 12.5 %all-to-all-start = ((bf16[8,8,128]{2,0,1:T(8,128)(2,1)}), bf16[8,8,128]{2,0,1:T(8,128)(2,1)S(1)}, u32[]{:S(2)}, u32[]{:S(2)}) async-start(bf16[8,8,128]{2,0,1:T(8,128)(2,1)} %fusion.33), calls=%async_computation | async-start | bytes 32768 | tf_op jit(solution)/shard_map/all_to_all | solution.py:89
  42.3 10.2 %all-to-all-start.1 = ((bf16[8,32,128]{2,1,0:T(8,128)(2,1)}), bf16[8,32,128]{2,1,0:T(8,128)(2,1)S(1)}, u32[]{:S(2)}, u32[]{:S(2)}) async-start(bf16[8,32,128]{2,1,0:T(8,128)(2,1)} %bitcast.18), calls=%async_computation.1 | async-start | bytes 131072 | tf_op jit(solution)/shard_map/all_to_all | solution.py:99
  45.7 1.2 %copy-start.9 = (f32[64,2]{0,1:T(2,128)S(1)}, f32[64,2]{0,1:T(2,128)}, u32[]{:S(2)}) copy-start(f32[64,2]{0,1:T(2,128)} %param.36) | copy-start | bytes 1540
  45.7 7.0 %copy-start.7 = (f32[1024]{0:T(1024)S(1)}, f32[1024]{0:T(1024)}, u32[]{:S(2)}) copy-start(f32[1024]{0:T(1024)} %param.34) | copy-start | bytes 12292
  45.7 7.3 %copy-start.6 = (bf16[1,1024,128]{2,1,0:T(8,128)(2,1)S(1)}, bf16[1,1024,128]{2,1,0:T(8,128)(2,1)}, u32[]{:S(2)}) copy-start(bf16[1,1024,128]{2,1,0:T(8,128)(2,1)} %param.38) | copy-start | bytes 786436
  46.9 5.9 %copy-start.4 = (bf16[1,1024,128]{2,1,0:T(8,128)(2,1)S(1)}, bf16[1,1024,128]{2,1,0:T(8,128)(2,1)}, u32[]{:S(2)}) copy-start(bf16[1,1024,128]{2,1,0:T(8,128)(2,1)} %param.37) | copy-start | bytes 786436
  52.7 1.0 %copy-start.5 = (bf16[1,128,1024]{2,1,0:T(8,128)(2,1)S(1)}, bf16[1,128,1024]{2,1,0:T(8,128)(2,1)}, u32[]{:S(2)}) copy-start(bf16[1,128,1024]{2,1,0:T(8,128)(2,1)} %param.39) | copy-start | bytes 786436
  63.9 10.2 %all-to-all-start.2 = ((bf16[8,2,2048]{2,1,0:T(2,128)(2,1)}), bf16[8,2,2048]{2,1,0:T(2,128)(2,1)S(1)}, u32[]{:S(2)}, u32[]{:S(2)}) async-start(bf16[8,2,2048]{2,1,0:T(2,128)(2,1)} %reshape.307), calls=%async_computation.2 | async-start | bytes 131072 | tf_op jit(solution)/shard_map/all_to_all | solution.py:110
